TPU v7x, 32 devices: a whole 2x2x4 slice. The times are simulated.
32 devices in a mesh: rep: 2 (over x), fs: 8 (over z, y), tp: 2 (over core).
Axes of the slice: x: 2, y: 2, z: 4, core: 2. Of those that a mesh axis runs over, the one named last changes fastest.
Arguments:
- tokens: bfloat16 [2048, 2048], P(('rep', 'fs')), may hold values from -6 to 6
- attention_norm_gain: float32 [2048], replicated, may hold values from 0.1 to 1.9
- query_weight: bfloat16 [2048, 1024], P('fs', 'tp'), may hold values from -0.125 to 0.125
- key_weight: bfloat16 [2048, 1024], P('fs', 'tp'), may hold values from -0.125 to 0.125
- value_weight: bfloat16 [2048, 2048], P('fs', 'tp'), may hold values from -0.125 to 0.125
- decay_weight: bfloat16 [2048, 1024], P('fs', 'tp'), may hold values from -0.125 to 0.125
- decay_gate_bias: float32 [1024], P('tp'), may hold values from -1.5 to 5.5
- decay_spike_extra: float32 [2048, 32], P(('rep', 'fs'), 'tp'), may hold values from -0.7 to 0
- head_output_gain: float32 [64], replicated, may hold values from 0.1 to 1.9
- output_weight: bfloat16 [2048, 2048], P('fs', 'tp'), may hold values from -0.125 to 0.125
- channel_norm_gain: float32 [2048], replicated, may hold values from 0.1 to 1.9
- gate_weight: bfloat16 [2048, 3072], P('fs', 'tp'), may hold values from -0.125 to 0.125
- up_weight: bfloat16 [2048, 3072], P('fs', 'tp'), may hold values from -0.125 to 0.125
- down_weight: bfloat16 [2048, 3072], P('fs', 'tp'), may hold values from -0.109375 to 0.109375
Outputs:
- layer_out: bfloat16 [2048, 2048], P(('rep', 'fs'))
All inputs are finite; a program needn't handle non-finite values.
Results may differ from a plain program's by a relative error of at most 0.018.
Values may be sent and summed in bfloat16 or wider, within the bound.
A program may use at most 128 MiB of HBM per device.

v0:
```python
import functools

import jax
import jax.numpy as jnp
import numpy as np
from jax import lax
from jax.experimental import pallas as pl
from jax.sharding import PartitionSpec as P

GATE_NORM = 16.0
NORM_EPS = 1e-06
LANES = 128


def rms_scale(values, scales):
    floats = values.astype(jnp.float32)
    return floats * lax.rsqrt(jnp.mean(floats * floats, axis=-1, keepdims=True) + NORM_EPS) * scales


def range_matrices(length):
    i = np.arange(length)[:, None]
    s = np.arange(length)[None, :]
    rows = []
    size = 2
    while size <= length:
        middle = i // size * size + size // 2
        late = i >= middle
        rows.append(np.where(late, (s >= middle) & (s <= i), (s >= i) & (s < middle)))
        rows.append(np.where(late, (s >= middle) & (s < i), (s > i) & (s < middle)))
        size *= 2
    return np.concatenate(rows, 0).astype(np.float32)


def attention_kernel(
    key_width, value_width, q_ref, k_ref, v_ref, g_ref, bias_ref, spike_ref, gain_ref, m_ref, o_ref
):
    length, lanes = q_ref.shape
    heads = lanes // key_width
    pre = g_ref[...] + bias_ref[...]
    log_sig = jnp.minimum(pre, 0.0) - jnp.log1p(jnp.exp(-jnp.abs(pre)))
    decay = log_sig / GATE_NORM + spike_ref[...]
    high = decay.astype(jnp.bfloat16)
    low = (decay - high.astype(jnp.float32)).astype(jnp.bfloat16)
    q = q_ref[...].astype(jnp.float32) * key_width ** (-0.5)
    k = k_ref[...].astype(jnp.float32)
    lane_head = lax.broadcasted_iota(jnp.int32, (length, lanes), 1) // key_width
    apart = lax.broadcasted_iota(jnp.int32, (length, length), 0) ^ lax.broadcasted_iota(
        jnp.int32, (length, length), 1
    )

    def scores(left, right, h):
        masked = jnp.where(lane_head == h, left, 0.0).astype(jnp.bfloat16)
        return lax.dot_general(
            masked, right, (((1,), (1,)), ((), ())), preferred_element_type=jnp.float32
        )

    def factor(index):
        part = m_ref[pl.ds(index * length, length), :]
        total = jnp.dot(part, high, preferred_element_type=jnp.float32)
        return jnp.exp(total + jnp.dot(part, low, preferred_element_type=jnp.float32))

    k_low = k.astype(jnp.bfloat16)
    acc = [2.0 * scores(q, k_low, h) for h in range(heads)]
    level, size = 0, 1
    while size < length:
        left = q * factor(2 * level)
        right = (k * factor(2 * level + 1)).astype(jnp.bfloat16)
        acc = [jnp.where(apart >= size, scores(left, right, h), acc[h]) for h in range(heads)]
        level, size = level + 1, size * 2
    per = min(heads, max(1, LANES // value_width))
    wide = per * value_width
    lane_value = lax.broadcasted_iota(jnp.int32, (length, wide), 1) // value_width
    for group in range(heads // per):
        span = slice(group * wide, (group + 1) * wide)
        values = v_ref[:, span]
        mixed = jnp.zeros((length, wide), jnp.float32)
        for n in range(per):
            one = jnp.dot(
                acc[group * per + n].astype(jnp.bfloat16), values, preferred_element_type=jnp.float32
            )
            mixed = jnp.where(lane_value == n, one, mixed)
        square = mixed * mixed
        scale = jnp.zeros((length, wide), jnp.float32)
        for n in range(per):
            mean = jnp.sum(jnp.where(lane_value == n, square, 0.0), -1, keepdims=True) / value_width
            scale = jnp.where(lane_value == n, lax.rsqrt(mean + NORM_EPS), scale)
        o_ref[:, span] = (mixed * scale * gain_ref[:, span]).astype(jnp.bfloat16)


def attention(length, key_width, value_width, q, k, v, gate, bias, spike, gain):
    rows, width = q.shape
    lanes = min(width, LANES)
    wide = lanes // key_width * value_width
    matrices = jnp.asarray(range_matrices(length), jnp.bfloat16)
    narrow_spec = pl.BlockSpec((length, lanes), lambda s, g: (s, g))
    wide_spec = pl.BlockSpec((length, wide), lambda s, g: (s, g))
    return pl.pallas_call(
        functools.partial(attention_kernel, key_width, value_width),
        grid=(rows // length, width // lanes),
        in_specs=[
            narrow_spec,
            narrow_spec,
            wide_spec,
            narrow_spec,
            pl.BlockSpec((1, lanes), lambda s, g: (0, g)),
            narrow_spec,
            pl.BlockSpec((1, wide), lambda s, g: (0, 0)),
            pl.BlockSpec(matrices.shape, lambda s, g: (0, 0)),
        ],
        out_specs=wide_spec,
        out_shape=jax.ShapeDtypeStruct(v.shape, jnp.bfloat16),
    )(q, k, v, gate, bias, spike, gain, matrices)


def make_shards(n_fs, n_tp):
    half_ring = n_fs // 2
    order = [2 * i for i in range(half_ring)] + [2 * i + 1 for i in reversed(range(half_ring))]
    ahead = [(order[i], order[(i + 1) % n_fs]) for i in range(n_fs)]
    behind = [(b, a) for a, b in ahead]
    swap = [(0, 1), (1, 0)]

    def position(f):
        return jnp.where(f % 2 == 0, f // 2, n_fs - 1 - f // 2)

    def member(p):
        return jnp.where(p < half_ring, 2 * p, 2 * (n_fs - 1 - p) + 1)

    def ring(block):
        out, back, front = [block], block, block
        for _ in range(1, half_ring):
            back = lax.ppermute(back, "fs", ahead)
            front = lax.ppermute(front, "fs", behind)
            out += [back, front]
        cut = block.shape[0] // 2
        back = lax.ppermute(back[:cut], "fs", ahead)
        front = lax.ppermute(front[cut:], "fs", behind)
        return out + [jnp.concatenate([back, front], 0)]

    def tp_scatter(total):
        if n_tp != 2:
            return lax.psum_scatter(
                total.astype(jnp.bfloat16), "tp", scatter_dimension=1, tiled=True
            ).astype(jnp.float32)
        c = lax.axis_index("tp")
        cut = total.shape[1] // 2
        mine = lax.dynamic_slice_in_dim(total, c * cut, cut, 1)
        other = lax.dynamic_slice_in_dim(total, (1 - c) * cut, cut, 1)
        return mine + lax.ppermute(other.astype(jnp.bfloat16), "tp", swap).astype(jnp.float32)

    def tp_gather(part):
        if n_tp != 2:
            return lax.all_gather(part, "tp", axis=1, tiled=True)
        other = lax.ppermute(part, "tp", swap)
        first = lax.axis_index("tp") == 0
        return jnp.concatenate([jnp.where(first, part, other), jnp.where(first, other, part)], 1)

    def shards(
        tokens,
        attention_norm_gain,
        query_weight,
        key_weight,
        value_weight,
        decay_weight,
        decay_gate_bias,
        decay_spike_extra,
        head_output_gain,
        output_weight,
        channel_norm_gain,
        gate_weight,
        up_weight,
        down_weight,
    ):
        r, f, c = lax.axis_index("rep"), lax.axis_index("fs"), lax.axis_index("tp")
        length, model = tokens.shape
        block = model // n_fs
        p = position(f)

        def own(weight, which=None, axis=1):
            cut = weight.shape[axis] // 2
            return lax.dynamic_slice_in_dim(weight, (r if which is None else which) * cut, cut, axis)

        shifts = [0]
        for d in range(1, half_ring):
            shifts += [n_fs - d, d]
        shifts += [half_ring]
        slots = [member((p + d) % n_fs) for d in shifts]

        def ring_order(array):
            axis = array.ndim - 1
            return jnp.concatenate(
                [lax.dynamic_slice_in_dim(array, s * block, block, axis) for s in slots], axis
            )

        def natural_order(array):
            pieces = []
            for j in range(n_fs):
                d = (order.index(j) - p) % n_fs
                slot = jnp.where(d > half_ring, 2 * (n_fs - d) - 1, 2 * d)
                slot = jnp.where(d == half_ring, n_fs - 1, slot)
                pieces.append(lax.dynamic_slice_in_dim(array, slot * block, block, 1))
            return jnp.concatenate(pieces, 1)

        def over_blocks(rows, blocks):
            total = None
            for s, weight in enumerate(blocks):
                term = jnp.dot(
                    rows[:, s * block : (s + 1) * block], weight, preferred_element_type=jnp.float32
                )
                total = term if total is None else total + term
            return total

        def to_features(rows, blocks):
            return jnp.concatenate(
                [
                    lax.dot_general(
                        rows, w, (((1,), (1,)), ((), ())), preferred_element_type=jnp.float32
                    )
                    for w in blocks
                ],
                1,
            )

        narrow = query_weight.shape[1] // 2
        wide = value_weight.shape[1] // 2
        heads = decay_spike_extra.shape[1] // 2
        key_width, value_width = narrow // heads, wide // heads
        first = ring(
            jnp.concatenate(
                [own(query_weight), own(key_weight), own(value_weight), own(decay_weight)], 1
            ),
        )
        outputs = ring(own(output_weight))
        gates = ring(own(gate_weight))
        ups = ring(own(up_weight))
        downs = ring(own(down_weight))

        mine = ring_order(tokens)
        both = jnp.concatenate([mine, lax.ppermute(mine, "rep", swap)], 0)
        spike = jnp.concatenate(
            [
                own(decay_spike_extra),
                lax.ppermute(own(decay_spike_extra, 1 - r), "rep", swap),
            ],
            0,
        )
        spike = jnp.repeat(spike, key_width, axis=1)
        bias = own(decay_gate_bias, axis=0)[None, :]
        group_heads = min(narrow, LANES) // key_width
        head_gain = jnp.tile(head_output_gain, group_heads)[None, :]

        normed = rms_scale(both, ring_order(attention_norm_gain)).astype(jnp.bfloat16)
        proj = over_blocks(normed, first)
        low = proj[:, : 2 * narrow + wide].astype(jnp.bfloat16)
        attended = attention(
            length,
            key_width,
            value_width,
            low[:, :narrow],
            low[:, narrow : 2 * narrow],
            low[:, 2 * narrow :],
            proj[:, 2 * narrow + wide :],
            bias,
            spike,
            head_gain,
        )
        mixer = tp_scatter(to_features(attended, outputs)).astype(jnp.bfloat16)
        turned = jnp.concatenate([mixer[length:], mixer[:length]], 0)
        turned = lax.ppermute(turned, "rep", swap)
        mixed = mixer.astype(jnp.float32) + turned.astype(jnp.float32)
        part = mixed.shape[1]
        residual_part = (
            lax.dynamic_slice_in_dim(both, c * part, part, 1).astype(jnp.float32) + mixed
        ).astype(jnp.bfloat16)
        residual = tp_gather(residual_part)
        normed_two = rms_scale(residual, ring_order(channel_norm_gain)).astype(jnp.bfloat16)
        gate_pre = over_blocks(normed_two, gates)
        up_pre = over_blocks(normed_two, ups)
        hidden = (jax.nn.silu(gate_pre) * up_pre).astype(jnp.bfloat16)
        split = n_fs - 3
        pieces = []
        for low_slot, high_slot in ((0, split), (split, n_fs)):
            channel = tp_scatter(to_features(hidden, downs[low_slot:high_slot]))
            channel = channel.astype(jnp.bfloat16)
            cut = channel.shape[1]
            other = lax.ppermute(channel[length:], "rep", swap).astype(jnp.float32)
            channel = channel[:length].astype(jnp.float32) + other
            start = low_slot * block + c * cut
            rest = lax.dynamic_slice_in_dim(residual[:length], start, cut, 1).astype(jnp.float32)
            pieces.append(tp_gather((rest + channel).astype(jnp.bfloat16)))
        return natural_order(jnp.concatenate(pieces, 1))

    return shards


def solution(mesh):
    in_specs = (
        P(("rep", "fs"), None),
        P(),
        P("fs", "tp"),
        P("fs", "tp"),
        P("fs", "tp"),
        P("fs", "tp"),
        P("tp"),
        P(("rep", "fs"), "tp"),
        P(),
        P("fs", "tp"),
        P(),
        P("fs", "tp"),
        P("fs", "tp"),
        P("fs", "tp"),
    )
    shards = make_shards(mesh.shape["fs"], mesh.shape["tp"])

    return jax.shard_map(
        shards,
        mesh=mesh,
        in_specs=in_specs,
        out_specs=P(("rep", "fs"), None),
        check_vma=False,
    )
```

profile of v0, /device:TPU:0, one launch (start us, length us, event | category | flops | bytes accessed | tf_op | source)
XLA Modules:
  0.0 230.5 jit_solution(6158244547927255461)
XLA Ops:
  1.0 3.1 %collective-permute-start.10 = (bf16[256,512]{1,0:T(8,128)(2,1)S(1)}, bf16[256,512]{1,0:T(8,128)(2,1)S(1)}, u32[]{:S(2)}, u32[]{:S(2)}) collective-permute-start(bf16[256,512]{1,0:T(8,128)(2,1)S(1)} %constant_dynamic-slice_fusion.3), channel_id=1, source_target_pairs={{0,4},{4,8},{8,12},{12,14},{14,10},{10,6},{6,2},{2,0},{1,5},{5,9},... | collective-permute-start | bytes 786440 | tf_op jit(solution)/shard_map/ppermute | solution.py:131
  6.4 2.0 collective-permute-start
  10.4 1.6 collective-permute-start.1
  20.1 1.7 collective-permute-start.2
  23.4 1.7 collective-permute-start.13
  33.4 7.7 %collective-permute-done.13 = bf16[256,512]{1,0:T(8,128)(2,1)} collective-permute-done((bf16[256,512]{1,0:T(8,128)(2,1)}, bf16[256,512]{1,0:T(8,128)(2,1)}, u32[]{:S(2)}, u32[]{:S(2)}) %collective-permute-start.13) | collective-permute-done | bytes 262176 | tf_op jit(solution)/shard_map/ppermute | solution.py:132
  42.9 1.6 collective-permute-start.4
  46.4 15.4 %collective-permute-done.4 = bf16[256,1280]{1,0:T(8,128)(2,1)S(1)} collective-permute-done((bf16[256,1280]{1,0:T(8,128)(2,1)}, bf16[256,1280]{1,0:T(8,128)(2,1)S(1)}, u32[]{:S(2)}, u32[]{:S(2)}) %collective-permute-start.4) | collective-permute-done | bytes 655392 | tf_op jit(solution)/shard_map/ppermute | solution.py:132
  70.6 10.0 %collective-permute-done.5 = bf16[256,1280]{1,0:T(8,128)(2,1)S(1)} collective-permute-done((bf16[256,1280]{1,0:T(8,128)(2,1)S(1)}, bf16[256,1280]{1,0:T(8,128)(2,1)S(1)}, u32[]{:S(2)}, u32[]{:S(2)}) %collective-permute-start.5) | collective-permute-done | bytes 655392 | tf_op jit(solution)/shard_map/ppermute | solution.py:131
  83.5 4.2 %collective-permute-done.7 = bf16[128,1280]{1,0:T(8,128)(2,1)S(1)} collective-permute-done((bf16[128,1280]{1,0:T(8,128)(2,1)S(1)}, bf16[128,1280]{1,0:T(8,128)(2,1)S(1)}, u32[]{:S(2)}, u32[]{:S(2)}) %collective-permute-start.7) | collective-permute-done | bytes 327712 | tf_op jit(solution)/shard_map/ppermute | solution.py:135
  91.6 11.1 %shard_map.145 = bf16[256,512]{1,0:T(8,128)(2,1)} custom-call(bf16[256,256]{1,0:T(8,128)(2,1)} %get-tuple-element.8.q_ref, bf16[256,256]{1,0:T(8,128)(2,1)} %get-tuple-element.7.k_ref, bf16[256,512]{1,0:T(8,128)(2,1)} %slice.174.v_ref, f32[256,256]{1,0:T(8,128)} %slice.175.g_ref, f32[1,256]{1,0:T(1,128)} %bitcast.53, f32[256,256]{1,0:T(8,128)} %copy.34.spike_ref, ...), custom_call_target="tpu_custom_call" | custom-call | tf_op jit(solution)/shard_map/pallas_call | solution.py:97
  121.8 3.3 %collective-permute-done.21 = bf16[256,768]{1,0:T(8,128)(2,1)} collective-permute-done((bf16[256,768]{1,0:T(8,128)(2,1)S(1)}, bf16[256,768]{1,0:T(8,128)(2,1)}, u32[]{:S(2)}, u32[]{:S(2)}) %collective-permute-start.21) | collective-permute-done | bytes 393248 | tf_op jit(solution)/shard_map/ppermute | solution.py:131
  127.6 5.9 %collective-permute-done.29 = bf16[256,768]{1,0:T(8,128)(2,1)} collective-permute-done((bf16[256,768]{1,0:T(8,128)(2,1)S(1)}, bf16[256,768]{1,0:T(8,128)(2,1)}, u32[]{:S(2)}, u32[]{:S(2)}) %collective-permute-start.29) | collective-permute-done | bytes 393248 | tf_op jit(solution)/shard_map/ppermute | solution.py:131
  134.6 1.6 collective-permute-start.23
  136.2 5.7 %collective-permute-done.37 = bf16[256,768]{1,0:T(8,128)(2,1)} collective-permute-done((bf16[256,768]{1,0:T(8,128)(2,1)S(1)}, bf16[256,768]{1,0:T(8,128)(2,1)}, u32[]{:S(2)}, u32[]{:S(2)}) %collective-permute-start.37) | collective-permute-done | bytes 393248 | tf_op jit(solution)/shard_map/ppermute | solution.py:131
  143.0 1.6 collective-permute-start.31
  144.7 6.8 %collective-permute-done.24 = bf16[256,768]{1,0:T(8,128)(2,1)} collective-permute-done((bf16[256,768]{1,0:T(8,128)(2,1)}, bf16[256,768]{1,0:T(8,128)(2,1)}, u32[]{:S(2)}, u32[]{:S(2)}) %collective-permute-start.24) | collective-permute-done | bytes 393248 | tf_op jit(solution)/shard_map/ppermute | solution.py:132
  153.5 6.3 %collective-permute-done.32 = bf16[256,768]{1,0:T(8,128)(2,1)S(1)} collective-permute-done((bf16[256,768]{1,0:T(8,128)(2,1)}, bf16[256,768]{1,0:T(8,128)(2,1)S(1)}, u32[]{:S(2)}, u32[]{:S(2)}) %collective-permute-start.32) | collective-permute-done | bytes 393248 | tf_op jit(solution)/shard_map/ppermute | solution.py:132
  163.5 3.6 %collective-permute-done.39 = bf16[256,768]{1,0:T(8,128)(2,1)} collective-permute-done((bf16[256,768]{1,0:T(8,128)(2,1)}, bf16[256,768]{1,0:T(8,128)(2,1)}, u32[]{:S(2)}, u32[]{:S(2)}) %collective-permute-start.39) | collective-permute-done | bytes 393248 | tf_op jit(solution)/shard_map/ppermute | solution.py:131
  169.9 5.6 %collective-permute-done.25 = bf16[256,768]{1,0:T(8,128)(2,1)S(1)} collective-permute-done((bf16[256,768]{1,0:T(8,128)(2,1)}, bf16[256,768]{1,0:T(8,128)(2,1)S(1)}, u32[]{:S(2)}, u32[]{:S(2)}) %collective-permute-start.25) | collective-permute-done | bytes 393248 | tf_op jit(solution)/shard_map/ppermute | solution.py:131
  178.9 5.0 %collective-permute-done.33 = bf16[256,768]{1,0:T(8,128)(2,1)S(1)} collective-permute-done((bf16[256,768]{1,0:T(8,128)(2,1)}, bf16[256,768]{1,0:T(8,128)(2,1)S(1)}, u32[]{:S(2)}, u32[]{:S(2)}) %collective-permute-start.33) | collective-permute-done | bytes 393248 | tf_op jit(solution)/shard_map/ppermute | solution.py:131
  186.0 6.3 %collective-permute-done.44 = bf16[256,768]{1,0:T(8,128)(2,1)S(1)} collective-permute-done((bf16[256,768]{1,0:T(8,128)(2,1)}, bf16[256,768]{1,0:T(8,128)(2,1)S(1)}, u32[]{:S(2)}, u32[]{:S(2)}) %collective-permute-start.44) | collective-permute-done | bytes 393248 | tf_op jit(solution)/shard_map/ppermute | solution.py:131
  221.3 3.5 %collective-permute-done.49 = bf16[128,384]{0,1:T(8,128)(2,1)S(1)} collective-permute-done((bf16[128,384]{0,1:T(8,128)(2,1)S(1)}, bf16[128,384]{0,1:T(8,128)(2,1)S(1)}, u32[]{:S(2)}, u32[]{:S(2)}) %collective-permute-start.49) | collective-permute-done | bytes 98336 | tf_op jit(solution)/shard_map/ppermute | solution.py:285
  224.9 2.8 %collective-permute-done.42 = bf16[128,640]{0,1:T(8,128)(2,1)S(1)} collective-permute-done((bf16[128,640]{0,1:T(8,128)(2,1)S(1)}, bf16[128,640]{0,1:T(8,128)(2,1)S(1)}, u32[]{:S(2)}, u32[]{:S(2)}) %collective-permute-start.42) | collective-permute-done | bytes 163872 | tf_op jit(solution)/shard_map/ppermute | solution.py:285
  (251 shorter events, 111.4 us)
Async XLA Ops:
  1.0 22.0 %collective-permute-start.10 = (bf16[256,512]{1,0:T(8,128)(2,1)S(1)}, bf16[256,512]{1,0:T(8,128)(2,1)S(1)}, u32[]{:S(2)}, u32[]{:S(2)}) collective-permute-start(bf16[256,512]{1,0:T(8,128)(2,1)S(1)} %constant_dynamic-slice_fusion.3), channel_id=1, source_target_pairs={{0,4},{4,8},{8,12},{12,14},{14,10},{10,6},{6,2},{2,0},{1,5},{5,9},... | collective-permute-start | bytes 786440 | tf_op jit(solution)/shard_map/ppermute | solution.py:131
  4.2 19.3 %collective-permute-start.11 = (bf16[256,512]{1,0:T(8,128)(2,1)S(1)}, bf16[256,512]{1,0:T(8,128)(2,1)}, u32[]{:S(2)}, u32[]{:S(2)}) collective-permute-start(bf16[256,512]{1,0:T(8,128)(2,1)S(1)} %constant_dynamic-slice_fusion.3), channel_id=1, source_target_pairs={{4,0},{8,4},{12,8},{14,12},{10,14},{6,10},{2,6},{0,2},{5,1},{9,5},... | collective-permute-start | bytes 786440 | tf_op jit(solution)/shard_map/ppermute | solution.py:132
  6.4 36.1 %collective-permute-start = (bf16[128,2048]{0,1:T(8,128)(2,1)S(1)}, bf16[128,2048]{0,1:T(8,128)(2,1)S(1)}, u32[]{:S(2)}, u32[]{:S(2)}) collective-permute-start(bf16[128,2048]{0,1:T(8,128)(2,1)S(1)} %constant_dynamic-update-slice_fusion), channel_id=1, source_target_pairs={{0,16},{16,0},{1,17},{17,1},{2,18},{18,2},{3,19},{19,3},{4,20},{20... | collective-permute-start | bytes 1572872 | tf_op jit(solution)/shard_map/ppermute | solution.py:238
  10.4 34.1 %collective-permute-start.1 = (bf16[256,1280]{1,0:T(8,128)(2,1)S(1)}, bf16[256,1280]{1,0:T(8,128)(2,1)}, u32[]{:S(2)}, u32[]{:S(2)}) collective-permute-start(bf16[256,1280]{1,0:T(8,128)(2,1)S(1)} %pad_maximum_fusion.3), channel_id=1, source_target_pairs={{0,4},{4,8},{8,12},{12,14},{14,10},{10,6},{6,2},{2,0},{1,5},{5,9},... | collective-permute-start | bytes 1966088 | tf_op jit(solution)/shard_map/ppermute | solution.py:131
  20.1 22.8 %collective-permute-start.2 = (bf16[256,1280]{1,0:T(8,128)(2,1)S(1)}, bf16[256,1280]{1,0:T(8,128)(2,1)}, u32[]{:S(2)}, u32[]{:S(2)}) collective-permute-start(bf16[256,1280]{1,0:T(8,128)(2,1)S(1)} %pad_maximum_fusion.3), channel_id=1, source_target_pairs={{4,0},{8,4},{12,8},{14,12},{10,14},{6,10},{2,6},{0,2},{5,1},{9,5},... | collective-permute-start | bytes 1966088 | tf_op jit(solution)/shard_map/ppermute | solution.py:132
  23.4 17.7 %collective-permute-start.13 = (bf16[256,512]{1,0:T(8,128)(2,1)}, bf16[256,512]{1,0:T(8,128)(2,1)}, u32[]{:S(2)}, u32[]{:S(2)}) collective-permute-start(bf16[256,512]{1,0:T(8,128)(2,1)} %collective-permute-done.11), channel_id=1, source_target_pairs={{4,0},{8,4},{12,8},{14,12},{10,14},{6,10},{2,6},{0,2},{5,1},{9,5},... | collective-permute-start | bytes 786440 | tf_op jit(solution)/shard_map/ppermute | solution.py:132
  32.0 34.8 %collective-permute-start.14 = (bf16[256,512]{1,0:T(8,128)(2,1)}, bf16[256,512]{1,0:T(8,128)(2,1)S(1)}, u32[]{:S(2)}, u32[]{:S(2)}) collective-permute-start(bf16[256,512]{1,0:T(8,128)(2,1)} %collective-permute-done.12), channel_id=1, source_target_pairs={{0,4},{4,8},{8,12},{12,14},{14,10},{10,6},{6,2},{2,0},{1,5},{5,9},... | collective-permute-start | bytes 786440 | tf_op jit(solution)/shard_map/ppermute | solution.py:131
  41.1 27.8 %collective-permute-start.15 = (bf16[256,512]{1,0:T(8,128)(2,1)}, bf16[256,512]{1,0:T(8,128)(2,1)S(1)}, u32[]{:S(2)}, u32[]{:S(2)}) collective-permute-start(bf16[256,512]{1,0:T(8,128)(2,1)} %collective-permute-done.13), channel_id=1, source_target_pairs={{4,0},{8,4},{12,8},{14,12},{10,14},{6,10},{2,6},{0,2},{5,1},{9,5},... | collective-permute-start | bytes 786440 | tf_op jit(solution)/shard_map/ppermute | solution.py:132
  42.9 19.0 %collective-permute-start.4 = (bf16[256,1280]{1,0:T(8,128)(2,1)}, bf16[256,1280]{1,0:T(8,128)(2,1)S(1)}, u32[]{:S(2)}, u32[]{:S(2)}) collective-permute-start(bf16[256,1280]{1,0:T(8,128)(2,1)} %collective-permute-done.2), channel_id=1, source_target_pairs={{4,0},{8,4},{12,8},{14,12},{10,14},{6,10},{2,6},{0,2},{5,1},{9,5},... | collective-permute-start | bytes 1966088 | tf_op jit(solution)/shard_map/ppermute | solution.py:132
  44.5 18.7 %collective-permute-start.3 = (bf16[256,1280]{1,0:T(8,128)(2,1)}, bf16[256,1280]{1,0:T(8,128)(2,1)S(1)}, u32[]{:S(2)}, u32[]{:S(2)}) collective-permute-start(bf16[256,1280]{1,0:T(8,128)(2,1)} %collective-permute-done.1), channel_id=1, source_target_pairs={{0,4},{4,8},{8,12},{12,14},{14,10},{10,6},{6,2},{2,0},{1,5},{5,9},... | collective-permute-start | bytes 1966088 | tf_op jit(solution)/shard_map/ppermute | solution.py:131
  61.8 19.7 %collective-permute-start.6 = (bf16[256,1280]{1,0:T(8,128)(2,1)S(1)}, bf16[256,1280]{1,0:T(8,128)(2,1)S(1)}, u32[]{:S(2)}, u32[]{:S(2)}) collective-permute-start(bf16[256,1280]{1,0:T(8,128)(2,1)S(1)} %collective-permute-done.4), channel_id=1, source_target_pairs={{4,0},{8,4},{12,8},{14,12},{10,14},{6,10},{2,6},{0,2},{5,1},{9,5},... | collective-permute-start | bytes 1966088 | tf_op jit(solution)/shard_map/ppermute | solution.py:132
  67.5 41.9 %collective-permute-start.16 = (bf16[128,512]{1,0:T(8,128)(2,1)}, bf16[128,512]{1,0:T(8,128)(2,1)}, u32[]{:S(2)}, u32[]{:S(2)}) collective-permute-start(bf16[128,512]{1,0:T(8,128)(2,1)} %slice.176), channel_id=1, source_target_pairs={{0,4},{4,8},{8,12},{12,14},{14,10},{10,6},{6,2},{2,0},{1,5},{5,9},... | collective-permute-start | bytes 393224 | tf_op jit(solution)/shard_map/ppermute | solution.py:135
  69.6 39.8 %collective-permute-start.17 = (bf16[128,512]{1,0:T(8,128)(2,1)}, bf16[128,512]{1,0:T(8,128)(2,1)}, u32[]{:S(2)}, u32[]{:S(2)}) collective-permute-start(bf16[128,512]{1,0:T(8,128)(2,1)} %slice.177), channel_id=1, source_target_pairs={{4,0},{8,4},{12,8},{14,12},{10,14},{6,10},{2,6},{0,2},{5,1},{9,5},... | collective-permute-start | bytes 393224 | tf_op jit(solution)/shard_map/ppermute | solution.py:136
  119.1 22.8 %collective-permute-start.37 = (bf16[256,768]{1,0:T(8,128)(2,1)S(1)}, bf16[256,768]{1,0:T(8,128)(2,1)}, u32[]{:S(2)}, u32[]{:S(2)}) collective-permute-start(bf16[256,768]{1,0:T(8,128)(2,1)S(1)} %constant_dynamic-slice_fusion), channel_id=1, source_target_pairs={{0,4},{4,8},{8,12},{12,14},{14,10},{10,6},{6,2},{2,0},{1,5},{5,9},... | collective-permute-start | bytes 1179656 | tf_op jit(solution)/shard_map/ppermute | solution.py:131
  125.0 36.3 %collective-permute-start.19 = (bf16[256,1024]{0,1:T(8,128)(2,1)S(1)}, bf16[256,1024]{0,1:T(8,128)(2,1)}, u32[]{:S(2)}, u32[]{:S(2)}) collective-permute-start(bf16[256,1024]{0,1:T(8,128)(2,1)S(1)} %pad_maximum_fusion.4), channel_id=1, source_target_pairs={{0,16},{16,0},{1,17},{17,1},{2,18},{18,2},{3,19},{19,3},{4,20},{20... | collective-permute-start | bytes 1572872 | tf_op jit(solution)/shard_map/ppermute | solution.py:268
  133.5 18.0 %collective-permute-start.24 = (bf16[256,768]{1,0:T(8,128)(2,1)}, bf16[256,768]{1,0:T(8,128)(2,1)}, u32[]{:S(2)}, u32[]{:S(2)}) collective-permute-start(bf16[256,768]{1,0:T(8,128)(2,1)} %collective-permute-done.22), channel_id=1, source_target_pairs={{4,0},{8,4},{12,8},{14,12},{10,14},{6,10},{2,6},{0,2},{5,1},{9,5},... | collective-permute-start | bytes 1179656 | tf_op jit(solution)/shard_map/ppermute | solution.py:132
  134.6 18.4 %collective-permute-start.23 = (bf16[256,768]{1,0:T(8,128)(2,1)}, bf16[256,768]{1,0:T(8,128)(2,1)}, u32[]{:S(2)}, u32[]{:S(2)}) collective-permute-start(bf16[256,768]{1,0:T(8,128)(2,1)} %collective-permute-done.21), channel_id=1, source_target_pairs={{0,4},{4,8},{8,12},{12,14},{14,10},{10,6},{6,2},{2,0},{1,5},{5,9},... | collective-permute-start | bytes 1179656 | tf_op jit(solution)/shard_map/ppermute | solution.py:131
  141.9 17.9 %collective-permute-start.32 = (bf16[256,768]{1,0:T(8,128)(2,1)}, bf16[256,768]{1,0:T(8,128)(2,1)S(1)}, u32[]{:S(2)}, u32[]{:S(2)}) collective-permute-start(bf16[256,768]{1,0:T(8,128)(2,1)} %collective-permute-done.30), channel_id=1, source_target_pairs={{4,0},{8,4},{12,8},{14,12},{10,14},{6,10},{2,6},{0,2},{5,1},{9,5},... | collective-permute-start | bytes 1179656 | tf_op jit(solution)/shard_map/ppermute | solution.py:132
  143.0 20.4 %collective-permute-start.31 = (bf16[256,768]{1,0:T(8,128)(2,1)}, bf16[256,768]{1,0:T(8,128)(2,1)}, u32[]{:S(2)}, u32[]{:S(2)}) collective-permute-start(bf16[256,768]{1,0:T(8,128)(2,1)} %collective-permute-done.29), channel_id=1, source_target_pairs={{0,4},{4,8},{8,12},{12,14},{14,10},{10,6},{6,2},{2,0},{1,5},{5,9},... | collective-permute-start | bytes 1179656 | tf_op jit(solution)/shard_map/ppermute | solution.py:131
  163.4 31.3 %collective-permute-start.20 = (bf16[256,1024]{0,1:T(8,128)(2,1)S(1)}, bf16[256,1024]{0,1:T(8,128)(2,1)S(1)}, u32[]{:S(2)}, u32[]{:S(2)}) collective-permute-start(bf16[256,1024]{0,1:T(8,128)(2,1)S(1)} %add_convert_fusion), channel_id=1, source_target_pairs={{0,1},{1,0},{2,3},{3,2},{4,5},{5,4},{6,7},{7,6},{8,9},{9,8},{10,11... | collective-permute-start | bytes 1572872 | tf_op jit(solution)/shard_map/ppermute | solution.py:153
  167.2 17.9 %collective-permute-start.34 = (bf16[256,768]{1,0:T(8,128)(2,1)S(1)}, bf16[256,768]{1,0:T(8,128)(2,1)S(1)}, u32[]{:S(2)}, u32[]{:S(2)}) collective-permute-start(bf16[256,768]{1,0:T(8,128)(2,1)S(1)} %copy-done.11), channel_id=1, source_target_pairs={{4,0},{8,4},{12,8},{14,12},{10,14},{6,10},{2,6},{0,2},{5,1},{9,5},... | collective-permute-start | bytes 1179656 | tf_op jit(solution)/shard_map/ppermute | solution.py:132
  183.9 24.4 %collective-permute-start.27 = (bf16[128,768]{1,0:T(8,128)(2,1)S(1)}, bf16[128,768]{1,0:T(8,128)(2,1)S(1)}, u32[]{:S(2)}, u32[]{:S(2)}) collective-permute-start(bf16[128,768]{1,0:T(8,128)(2,1)S(1)} %slice.190), channel_id=1, source_target_pairs={{0,4},{4,8},{8,12},{12,14},{14,10},{10,6},{6,2},{2,0},{1,5},{5,9},... | collective-permute-start | bytes 589832 | tf_op jit(solution)/shard_map/ppermute | solution.py:135
  185.1 24.2 %collective-permute-start.28 = (bf16[128,768]{1,0:T(8,128)(2,1)S(1)}, bf16[128,768]{1,0:T(8,128)(2,1)S(1)}, u32[]{:S(2)}, u32[]{:S(2)}) collective-permute-start(bf16[128,768]{1,0:T(8,128)(2,1)S(1)} %slice.191), channel_id=1, source_target_pairs={{4,0},{8,4},{12,8},{14,12},{10,14},{6,10},{2,6},{0,2},{5,1},{9,5},... | collective-permute-start | bytes 589832 | tf_op jit(solution)/shard_map/ppermute | solution.py:136
  194.7 22.2 %collective-permute-start.46 = (bf16[128,768]{1,0:T(8,128)(2,1)S(1)}, bf16[128,768]{1,0:T(8,128)(2,1)S(1)}, u32[]{:S(2)}, u32[]{:S(2)}) collective-permute-start(bf16[128,768]{1,0:T(8,128)(2,1)S(1)} %slice.196), channel_id=1, source_target_pairs={{0,4},{4,8},{8,12},{12,14},{14,10},{10,6},{6,2},{2,0},{1,5},{5,9},... | collective-permute-start | bytes 589832 | tf_op jit(solution)/shard_map/ppermute | solution.py:135
  (45 other events, 538.9 us)
where the time goes:
time: 232 us; the launch traced here: 230 us
  waiting for transfers between devices  96.4 us (42%)
  starting transfers between devices  53.3 us (23%)
  matrix products  32.4 us (14%)
  local copies, waits for them, and re-layouts  30.2 us (13%)
  Pallas kernels  11.1 us (5%)
  other arithmetic  5.94 us (3%)
    ppermute x15, waiting for transfers between devices, ring(): back = lax.ppermute(back, 'fs', ahead)  45.4 us
    ppermute x15, waiting for transfers between devices, ring(): front = lax.ppermute(front, 'fs', behind)  36.6 us
    ppermute x15, starting transfers between devices, ring(): back = lax.ppermute(back, 'fs', ahead)  20.1 us
    dot_general x24, matrix products, over_blocks(): jnp.dot(rows[:, s * block:(s + 1) * block], weight, preferred_element_typ...  18.2 us
    ppermute x15, starting transfers between devices, ring(): front = lax.ppermute(front, 'fs', behind)  16 us
    dot_general x16, matrix products, to_features(): lax.dot_general(rows, w, (((1,), (1,)), ((), ())), preferred_element_type...  14.2 us
    unnamed x71, local copies, waits for them, and re-layouts  12.6 us
    pallas_call x1, Pallas kernels, attention(): pl.pallas_call(functools.partial(attention_kernel, key_width, value_width...  11.1 us
  transfers between devices with their start and end apart: 51, of which 24 were waited for; matrix products, arithmetic and copies ran while one was open for 27% of the time, Pallas kernels for 5%

commit v1 on v0

--- a/solution.py
+++ b/solution.py
@@ -136,6 +136,21 @@
         front = lax.ppermute(front[cut:], "fs", behind)
         return out + [jnp.concatenate([back, front], 0)]
 
+    def halves_ring(block, names):
+        cut = block.shape[0] // 2
+        parts = []
+        for name, part in zip(names, (block[:cut], block[cut:])):
+            out, back, front = [part], part, part
+            for step in range(1, half_ring + 1):
+                if step < half_ring or name == names[0]:
+                    back = lax.ppermute(back, "fs", ahead)
+                if step < half_ring or name == names[1]:
+                    front = lax.ppermute(front, "fs", behind)
+                if step < half_ring:
+                    out += [back, front]
+            parts.append(out + [back if name == names[0] else front])
+        return [half for pair in zip(*parts) for half in pair]
+
     def tp_scatter(total):
         if n_tp != 2:
             return lax.psum_scatter(
@@ -204,21 +219,22 @@
             total = None
             for s, weight in enumerate(blocks):
                 term = jnp.dot(
-                    rows[:, s * block : (s + 1) * block], weight, preferred_element_type=jnp.float32
+                    rows[:, s * block : (s + 1) * block],
+                    weight,
+                    preferred_element_type=jnp.float32,
                 )
                 total = term if total is None else total + term
             return total
 
         def to_features(rows, blocks):
-            return jnp.concatenate(
-                [
+            terms = []
+            for weight in blocks:
+                terms.append(
                     lax.dot_general(
-                        rows, w, (((1,), (1,)), ((), ())), preferred_element_type=jnp.float32
+                        rows, weight, (((1,), (1,)), ((), ())), preferred_element_type=jnp.float32
                     )
-                    for w in blocks
-                ],
-                1,
-            )
+                )
+            return jnp.concatenate(terms, 1)
 
         narrow = query_weight.shape[1] // 2
         wide = value_weight.shape[1] // 2
@@ -232,7 +248,7 @@
         outputs = ring(own(output_weight))
         gates = ring(own(gate_weight))
         ups = ring(own(up_weight))
-        downs = ring(own(down_weight))
+        downs = halves_ring(own(down_weight), "dh")
 
         mine = ring_order(tokens)
         both = jnp.concatenate([mine, lax.ppermute(mine, "rep", swap)], 0)
@@ -263,11 +279,12 @@
             spike,
             head_gain,
         )
-        mixer = tp_scatter(to_features(attended, outputs)).astype(jnp.bfloat16)
+        mixer = to_features(attended, outputs)
+        mixer = tp_scatter(mixer).astype(jnp.bfloat16)
         turned = jnp.concatenate([mixer[length:], mixer[:length]], 0)
         turned = lax.ppermute(turned, "rep", swap)
+        part = mixer.shape[1]
         mixed = mixer.astype(jnp.float32) + turned.astype(jnp.float32)
-        part = mixed.shape[1]
         residual_part = (
             lax.dynamic_slice_in_dim(both, c * part, part, 1).astype(jnp.float32) + mixed
         ).astype(jnp.bfloat16)
@@ -279,7 +296,7 @@
         split = n_fs - 3
         pieces = []
         for low_slot, high_slot in ((0, split), (split, n_fs)):
-            channel = tp_scatter(to_features(hidden, downs[low_slot:high_slot]))
+            channel = tp_scatter(to_features(hidden, downs[2 * low_slot : 2 * high_slot]))
             channel = channel.astype(jnp.bfloat16)
             cut = channel.shape[1]
             other = lax.ppermute(channel[length:], "rep", swap).astype(jnp.float32)

time: 232 us -> 233 us (level)
  starting transfers between devices: 53.3 us -> 57 us
  matrix products: 32.4 us -> 29.8 us
    ppermute x0 -> x14, starting transfers between devices: none -> 14.4 us  [the longest x7 8.5 us: halves_ring(): back = lax.ppermute(back, 'fs', ahead)]
    ppermute x15 -> x12, waiting for transfers between devices: 36.6 us -> 23.2 us  [ring(): front = lax.ppermute(front, 'fs', behind)]
    ppermute x0 -> x14, waiting for transfers between devices: none -> 9.44 us  [the longest x7 5.2 us: halves_ring(): front = lax.ppermute(front, 'fs', behind)]
    ppermute x15 -> x12, starting transfers between devices: 20.1 us -> 14.5 us  [ring(): back = lax.ppermute(back, 'fs', ahead)]
    ppermute x5 -> x4, waiting for transfers between devices: 1.05 us -> 5.67 us  [ring(): front = lax.ppermute(front[cut:], 'fs', behind)]
    ppermute x15 -> x12, starting transfers between devices: 16 us -> 12.8 us  [ring(): front = lax.ppermute(front, 'fs', behind)]
    dot_general x16 -> x24, matrix products: 14.2 us -> 12.5 us  [to_features(): lax.dot_general(rows, weight, (((1,), (1,)), ((), ())), preferred_element...]
    ppermute x5 -> x4, starting transfers between devices: 4.71 us -> 3.55 us  [ring(): front = lax.ppermute(front[cut:], 'fs', behind)]
  transfers between devices with their start and end apart: 51 -> 57, of which waited for: 24 -> 22; matrix products, arithmetic and copies ran while one was open for 27% -> 26% of each run, Pallas kernels for 5% -> 5%
where the time goes in v1:
time: 233 us; the launch traced here: 231 us
  waiting for transfers between devices  95.9 us (41%)
  starting transfers between devices  57 us (24%)
  local copies, waits for them, and re-layouts  31.6 us (14%)
  matrix products  29.8 us (13%)
  Pallas kernels  11.1 us (5%)
  other arithmetic  4.79 us (2%)
    ppermute x12, waiting for transfers between devices, ring(): back = lax.ppermute(back, 'fs', ahead)  44.3 us
    ppermute x12, waiting for transfers between devices, ring(): front = lax.ppermute(front, 'fs', behind)  23.2 us
    dot_general x24, matrix products, over_blocks(): jnp.dot(rows[:, s * block:(s + 1) * block], weight, preferred_element_typ...  17.3 us
    ppermute x12, starting transfers between devices, ring(): back = lax.ppermute(back, 'fs', ahead)  14.5 us
    unnamed x73, local copies, waits for them, and re-layouts  13.3 us
    ppermute x12, starting transfers between devices, ring(): front = lax.ppermute(front, 'fs', behind)  12.8 us
    dot_general x24, matrix products, to_features(): lax.dot_general(rows, weight, (((1,), (1,)), ((), ())), preferred_element...  12.5 us
    pallas_call x1, Pallas kernels, attention(): pl.pallas_call(functools.partial(attention_kernel, key_width, value_width...  11.1 us
  transfers between devices with their start and end apart: 57, of which 22 were waited for; matrix products, arithmetic and copies ran while one was open for 26% of the time, Pallas kernels for 5%

profile of v1, /device:TPU:0, one launch (start us, length us, event | category | flops | bytes accessed | tf_op | source)
XLA Modules:
  0.0 231.4 jit_solution(4980894904042881452)
XLA Ops:
  1.0 3.1 %collective-permute-start.10 = (bf16[256,512]{1,0:T(8,128)(2,1)S(1)}, bf16[256,512]{1,0:T(8,128)(2,1)S(1)}, u32[]{:S(2)}, u32[]{:S(2)}) collective-permute-start(bf16[256,512]{1,0:T(8,128)(2,1)S(1)} %constant_dynamic-slice_fusion.2), channel_id=1, source_target_pairs={{0,4},{4,8},{8,12},{12,14},{14,10},{10,6},{6,2},{2,0},{1,5},{5,9},... | collective-permute-start | bytes 786440 | tf_op jit(solution)/shard_map/ppermute | solution.py:131
  6.4 2.0 collective-permute-start
  10.5 1.6 collective-permute-start.1
  20.0 1.7 collective-permute-start.2
  23.4 1.7 collective-permute-start.13
  33.5 7.6 %collective-permute-done.13 = bf16[256,512]{1,0:T(8,128)(2,1)} collective-permute-done((bf16[256,512]{1,0:T(8,128)(2,1)}, bf16[256,512]{1,0:T(8,128)(2,1)}, u32[]{:S(2)}, u32[]{:S(2)}) %collective-permute-start.13) | collective-permute-done | bytes 262176 | tf_op jit(solution)/shard_map/ppermute | solution.py:132
  42.9 1.6 collective-permute-start.4
  46.4 15.4 %collective-permute-done.4 = bf16[256,1280]{1,0:T(8,128)(2,1)S(1)} collective-permute-done((bf16[256,1280]{1,0:T(8,128)(2,1)}, bf16[256,1280]{1,0:T(8,128)(2,1)S(1)}, u32[]{:S(2)}, u32[]{:S(2)}) %collective-permute-start.4) | collective-permute-done | bytes 655392 | tf_op jit(solution)/shard_map/ppermute | solution.py:132
  70.5 10.0 %collective-permute-done.5 = bf16[256,1280]{1,0:T(8,128)(2,1)S(1)} collective-permute-done((bf16[256,1280]{1,0:T(8,128)(2,1)S(1)}, bf16[256,1280]{1,0:T(8,128)(2,1)S(1)}, u32[]{:S(2)}, u32[]{:S(2)}) %collective-permute-start.5) | collective-permute-done | bytes 655392 | tf_op jit(solution)/shard_map/ppermute | solution.py:131
  83.5 4.2 %collective-permute-done.7 = bf16[128,1280]{1,0:T(8,128)(2,1)S(1)} collective-permute-done((bf16[128,1280]{1,0:T(8,128)(2,1)S(1)}, bf16[128,1280]{1,0:T(8,128)(2,1)S(1)}, u32[]{:S(2)}, u32[]{:S(2)}) %collective-permute-start.7) | collective-permute-done | bytes 327712 | tf_op jit(solution)/shard_map/ppermute | solution.py:135
  91.7 11.1 %shard_map.145 = bf16[256,512]{1,0:T(8,128)(2,1)} custom-call(bf16[256,256]{1,0:T(8,128)(2,1)} %get-tuple-element.10.q_ref, bf16[256,256]{1,0:T(8,128)(2,1)} %get-tuple-element.9.k_ref, bf16[256,512]{1,0:T(8,128)(2,1)} %slice.174.v_ref, f32[256,256]{1,0:T(8,128)} %slice.175.g_ref, f32[1,256]{1,0:T(1,128)} %bitcast.70, f32[256,256]{1,0:T(8,128)} %copy.34.spike_ref, ...), custom_call_target="tpu_custom_call" | custom-call | tf_op jit(solution)/shard_map/pallas_call | solution.py:97
  120.6 4.3 %collective-permute-done.21 = bf16[256,768]{1,0:T(8,128)(2,1)S(1)} collective-permute-done((bf16[256,768]{1,0:T(8,128)(2,1)S(1)}, bf16[256,768]{1,0:T(8,128)(2,1)S(1)}, u32[]{:S(2)}, u32[]{:S(2)}) %collective-permute-start.21) | collective-permute-done | bytes 393248 | tf_op jit(solution)/shard_map/ppermute | solution.py:131
  127.1 6.4 %collective-permute-done.29 = bf16[256,768]{1,0:T(8,128)(2,1)} collective-permute-done((bf16[256,768]{1,0:T(8,128)(2,1)S(1)}, bf16[256,768]{1,0:T(8,128)(2,1)}, u32[]{:S(2)}, u32[]{:S(2)}) %collective-permute-start.29) | collective-permute-done | bytes 393248 | tf_op jit(solution)/shard_map/ppermute | solution.py:131
  135.8 6.1 %collective-permute-done.23 = bf16[256,768]{1,0:T(8,128)(2,1)} collective-permute-done((bf16[256,768]{1,0:T(8,128)(2,1)S(1)}, bf16[256,768]{1,0:T(8,128)(2,1)}, u32[]{:S(2)}, u32[]{:S(2)}) %collective-permute-start.23) | collective-permute-done | bytes 393248 | tf_op jit(solution)/shard_map/ppermute | solution.py:131
  143.9 6.4 %collective-permute-done.31 = bf16[256,768]{1,0:T(8,128)(2,1)} collective-permute-done((bf16[256,768]{1,0:T(8,128)(2,1)}, bf16[256,768]{1,0:T(8,128)(2,1)}, u32[]{:S(2)}, u32[]{:S(2)}) %collective-permute-start.31) | collective-permute-done | bytes 393248 | tf_op jit(solution)/shard_map/ppermute | solution.py:131
  154.1 4.6 %collective-permute-done.25 = bf16[256,768]{1,0:T(8,128)(2,1)S(1)} collective-permute-done((bf16[256,768]{1,0:T(8,128)(2,1)}, bf16[256,768]{1,0:T(8,128)(2,1)S(1)}, u32[]{:S(2)}, u32[]{:S(2)}) %collective-permute-start.25) | collective-permute-done | bytes 393248 | tf_op jit(solution)/shard_map/ppermute | solution.py:131
  160.7 6.5 %collective-permute-done.33 = bf16[256,768]{1,0:T(8,128)(2,1)} collective-permute-done((bf16[256,768]{1,0:T(8,128)(2,1)}, bf16[256,768]{1,0:T(8,128)(2,1)}, u32[]{:S(2)}, u32[]{:S(2)}) %collective-permute-start.33) | collective-permute-done | bytes 393248 | tf_op jit(solution)/shard_map/ppermute | solution.py:131
  170.8 4.2 %collective-permute-done.37 = bf16[128,768]{1,0:T(8,128)(2,1)S(1)} collective-permute-done((bf16[128,768]{1,0:T(8,128)(2,1)S(1)}, bf16[128,768]{1,0:T(8,128)(2,1)S(1)}, u32[]{:S(2)}, u32[]{:S(2)}) %collective-permute-start.37) | collective-permute-done | bytes 196640 | tf_op jit(solution)/shard_map/ppermute | solution.py:146
  196.1 2.4 %collective-permute-done.28 = bf16[128,768]{1,0:T(8,128)(2,1)S(1)} collective-permute-done((bf16[128,768]{1,0:T(8,128)(2,1)S(1)}, bf16[128,768]{1,0:T(8,128)(2,1)S(1)}, u32[]{:S(2)}, u32[]{:S(2)}) %collective-permute-start.28) | collective-permute-done | bytes 196640 | tf_op jit(solution)/shard_map/ppermute | solution.py:136
  199.8 3.0 %collective-permute-done.43 = bf16[128,768]{1,0:T(8,128)(2,1)S(1)} collective-permute-done((bf16[128,768]{1,0:T(8,128)(2,1)S(1)}, bf16[128,768]{1,0:T(8,128)(2,1)S(1)}, u32[]{:S(2)}, u32[]{:S(2)}) %collective-permute-start.43) | collective-permute-done | bytes 196640 | tf_op jit(solution)/shard_map/ppermute | solution.py:148
  204.8 2.2 collective-permute-done.51
  209.0 2.2 collective-permute-done.36
  222.1 3.5 %collective-permute-done.55 = bf16[128,384]{0,1:T(8,128)(2,1)S(1)} collective-permute-done((bf16[128,384]{0,1:T(8,128)(2,1)S(1)}, bf16[128,384]{0,1:T(8,128)(2,1)S(1)}, u32[]{:S(2)}, u32[]{:S(2)}) %collective-permute-start.55) | collective-permute-done | bytes 98336 | tf_op jit(solution)/shard_map/ppermute | solution.py:302
  225.7 2.8 %collective-permute-done.46 = bf16[128,640]{0,1:T(8,128)(2,1)S(1)} collective-permute-done((bf16[128,640]{0,1:T(8,128)(2,1)S(1)}, bf16[128,640]{0,1:T(8,128)(2,1)S(1)}, u32[]{:S(2)}, u32[]{:S(2)}) %collective-permute-start.46) | collective-permute-done | bytes 163872 | tf_op jit(solution)/shard_map/ppermute | solution.py:302
  (270 shorter events, 115.7 us)
Async XLA Ops:
  1.0 22.0 %collective-permute-start.10 = (bf16[256,512]{1,0:T(8,128)(2,1)S(1)}, bf16[256,512]{1,0:T(8,128)(2,1)S(1)}, u32[]{:S(2)}, u32[]{:S(2)}) collective-permute-start(bf16[256,512]{1,0:T(8,128)(2,1)S(1)} %constant_dynamic-slice_fusion.2), channel_id=1, source_target_pairs={{0,4},{4,8},{8,12},{12,14},{14,10},{10,6},{6,2},{2,0},{1,5},{5,9},... | collective-permute-start | bytes 786440 | tf_op jit(solution)/shard_map/ppermute | solution.py:131
  4.2 19.3 %collective-permute-start.11 = (bf16[256,512]{1,0:T(8,128)(2,1)S(1)}, bf16[256,512]{1,0:T(8,128)(2,1)}, u32[]{:S(2)}, u32[]{:S(2)}) collective-permute-start(bf16[256,512]{1,0:T(8,128)(2,1)S(1)} %constant_dynamic-slice_fusion.2), channel_id=1, source_target_pairs={{4,0},{8,4},{12,8},{14,12},{10,14},{6,10},{2,6},{0,2},{5,1},{9,5},... | collective-permute-start | bytes 786440 | tf_op jit(solution)/shard_map/ppermute | solution.py:132
  6.4 36.1 %collective-permute-start = (bf16[128,2048]{0,1:T(8,128)(2,1)S(1)}, bf16[128,2048]{0,1:T(8,128)(2,1)S(1)}, u32[]{:S(2)}, u32[]{:S(2)}) collective-permute-start(bf16[128,2048]{0,1:T(8,128)(2,1)S(1)} %constant_dynamic-update-slice_fusion), channel_id=1, source_target_pairs={{0,16},{16,0},{1,17},{17,1},{2,18},{18,2},{3,19},{19,3},{4,20},{20... | collective-permute-start | bytes 1572872 | tf_op jit(solution)/shard_map/ppermute | solution.py:254
  10.5 34.0 %collective-permute-start.1 = (bf16[256,1280]{1,0:T(8,128)(2,1)S(1)}, bf16[256,1280]{1,0:T(8,128)(2,1)}, u32[]{:S(2)}, u32[]{:S(2)}) collective-permute-start(bf16[256,1280]{1,0:T(8,128)(2,1)S(1)} %pad_maximum_fusion.2), channel_id=1, source_target_pairs={{0,4},{4,8},{8,12},{12,14},{14,10},{10,6},{6,2},{2,0},{1,5},{5,9},... | collective-permute-start | bytes 1966088 | tf_op jit(solution)/shard_map/ppermute | solution.py:131
  20.0 22.8 %collective-permute-start.2 = (bf16[256,1280]{1,0:T(8,128)(2,1)S(1)}, bf16[256,1280]{1,0:T(8,128)(2,1)}, u32[]{:S(2)}, u32[]{:S(2)}) collective-permute-start(bf16[256,1280]{1,0:T(8,128)(2,1)S(1)} %pad_maximum_fusion.2), channel_id=1, source_target_pairs={{4,0},{8,4},{12,8},{14,12},{10,14},{6,10},{2,6},{0,2},{5,1},{9,5},... | collective-permute-start | bytes 1966088 | tf_op jit(solution)/shard_map/ppermute | solution.py:132
  23.4 17.7 %collective-permute-start.13 = (bf16[256,512]{1,0:T(8,128)(2,1)}, bf16[256,512]{1,0:T(8,128)(2,1)}, u32[]{:S(2)}, u32[]{:S(2)}) collective-permute-start(bf16[256,512]{1,0:T(8,128)(2,1)} %collective-permute-done.11), channel_id=1, source_target_pairs={{4,0},{8,4},{12,8},{14,12},{10,14},{6,10},{2,6},{0,2},{5,1},{9,5},... | collective-permute-start | bytes 786440 | tf_op jit(solution)/shard_map/ppermute | solution.py:132
  32.0 34.8 %collective-permute-start.14 = (bf16[256,512]{1,0:T(8,128)(2,1)}, bf16[256,512]{1,0:T(8,128)(2,1)S(1)}, u32[]{:S(2)}, u32[]{:S(2)}) collective-permute-start(bf16[256,512]{1,0:T(8,128)(2,1)} %collective-permute-done.12), channel_id=1, source_target_pairs={{0,4},{4,8},{8,12},{12,14},{14,10},{10,6},{6,2},{2,0},{1,5},{5,9},... | collective-permute-start | bytes 786440 | tf_op jit(solution)/shard_map/ppermute | solution.py:131
  41.1 27.8 %collective-permute-start.15 = (bf16[256,512]{1,0:T(8,128)(2,1)}, bf16[256,512]{1,0:T(8,128)(2,1)S(1)}, u32[]{:S(2)}, u32[]{:S(2)}) collective-permute-start(bf16[256,512]{1,0:T(8,128)(2,1)} %collective-permute-done.13), channel_id=1, source_target_pairs={{4,0},{8,4},{12,8},{14,12},{10,14},{6,10},{2,6},{0,2},{5,1},{9,5},... | collective-permute-start | bytes 786440 | tf_op jit(solution)/shard_map/ppermute | solution.py:132
  42.9 19.0 %collective-permute-start.4 = (bf16[256,1280]{1,0:T(8,128)(2,1)}, bf16[256,1280]{1,0:T(8,128)(2,1)S(1)}, u32[]{:S(2)}, u32[]{:S(2)}) collective-permute-start(bf16[256,1280]{1,0:T(8,128)(2,1)} %collective-permute-done.2), channel_id=1, source_target_pairs={{4,0},{8,4},{12,8},{14,12},{10,14},{6,10},{2,6},{0,2},{5,1},{9,5},... | collective-permute-start | bytes 1966088 | tf_op jit(solution)/shard_map/ppermute | solution.py:132
  44.5 18.7 %collective-permute-start.3 = (bf16[256,1280]{1,0:T(8,128)(2,1)}, bf16[256,1280]{1,0:T(8,128)(2,1)S(1)}, u32[]{:S(2)}, u32[]{:S(2)}) collective-permute-start(bf16[256,1280]{1,0:T(8,128)(2,1)} %collective-permute-done.1), channel_id=1, source_target_pairs={{0,4},{4,8},{8,12},{12,14},{14,10},{10,6},{6,2},{2,0},{1,5},{5,9},... | collective-permute-start | bytes 1966088 | tf_op jit(solution)/shard_map/ppermute | solution.py:131
  61.8 19.7 %collective-permute-start.6 = (bf16[256,1280]{1,0:T(8,128)(2,1)S(1)}, bf16[256,1280]{1,0:T(8,128)(2,1)S(1)}, u32[]{:S(2)}, u32[]{:S(2)}) collective-permute-start(bf16[256,1280]{1,0:T(8,128)(2,1)S(1)} %collective-permute-done.4), channel_id=1, source_target_pairs={{4,0},{8,4},{12,8},{14,12},{10,14},{6,10},{2,6},{0,2},{5,1},{9,5},... | collective-permute-start | bytes 1966088 | tf_op jit(solution)/shard_map/ppermute | solution.py:132
  63.2 17.3 %collective-permute-start.5 = (bf16[256,1280]{1,0:T(8,128)(2,1)S(1)}, bf16[256,1280]{1,0:T(8,128)(2,1)S(1)}, u32[]{:S(2)}, u32[]{:S(2)}) collective-permute-start(bf16[256,1280]{1,0:T(8,128)(2,1)S(1)} %collective-permute-done.3), channel_id=1, source_target_pairs={{0,4},{4,8},{8,12},{12,14},{14,10},{10,6},{6,2},{2,0},{1,5},{5,9},... | collective-permute-start | bytes 1966088 | tf_op jit(solution)/shard_map/ppermute | solution.py:131
  67.5 42.0 %collective-permute-start.16 = (bf16[128,512]{1,0:T(8,128)(2,1)}, bf16[128,512]{1,0:T(8,128)(2,1)}, u32[]{:S(2)}, u32[]{:S(2)}) collective-permute-start(bf16[128,512]{1,0:T(8,128)(2,1)} %slice.176), channel_id=1, source_target_pairs={{0,4},{4,8},{8,12},{12,14},{14,10},{10,6},{6,2},{2,0},{1,5},{5,9},... | collective-permute-start | bytes 393224 | tf_op jit(solution)/shard_map/ppermute | solution.py:135
  69.6 39.9 %collective-permute-start.17 = (bf16[128,512]{1,0:T(8,128)(2,1)}, bf16[128,512]{1,0:T(8,128)(2,1)}, u32[]{:S(2)}, u32[]{:S(2)}) collective-permute-start(bf16[128,512]{1,0:T(8,128)(2,1)} %slice.177), channel_id=1, source_target_pairs={{4,0},{8,4},{12,8},{14,12},{10,14},{6,10},{2,6},{0,2},{5,1},{9,5},... | collective-permute-start | bytes 393224 | tf_op jit(solution)/shard_map/ppermute | solution.py:136
  116.0 17.5 %collective-permute-start.29 = (bf16[256,768]{1,0:T(8,128)(2,1)S(1)}, bf16[256,768]{1,0:T(8,128)(2,1)}, u32[]{:S(2)}, u32[]{:S(2)}) collective-permute-start(bf16[256,768]{1,0:T(8,128)(2,1)S(1)} %constant_dynamic-slice_fusion), channel_id=1, source_target_pairs={{0,4},{4,8},{8,12},{12,14},{14,10},{10,6},{6,2},{2,0},{1,5},{5,9},... | collective-permute-start | bytes 1179656 | tf_op jit(solution)/shard_map/ppermute | solution.py:131
  118.6 32.8 %collective-permute-start.19 = (bf16[256,1024]{0,1:T(8,128)(2,1)S(1)}, bf16[256,1024]{0,1:T(8,128)(2,1)S(1)}, u32[]{:S(2)}, u32[]{:S(2)}) collective-permute-start(bf16[256,1024]{0,1:T(8,128)(2,1)S(1)} %pad_maximum_fusion.3), channel_id=1, source_target_pairs={{0,16},{16,0},{1,17},{17,1},{2,18},{18,2},{3,19},{19,3},{4,20},{20... | collective-permute-start | bytes 1572872 | tf_op jit(solution)/shard_map/ppermute | solution.py:285
  124.9 17.0 %collective-permute-start.23 = (bf16[256,768]{1,0:T(8,128)(2,1)S(1)}, bf16[256,768]{1,0:T(8,128)(2,1)}, u32[]{:S(2)}, u32[]{:S(2)}) collective-permute-start(bf16[256,768]{1,0:T(8,128)(2,1)S(1)} %collective-permute-done.21), channel_id=1, source_target_pairs={{0,4},{4,8},{8,12},{12,14},{14,10},{10,6},{6,2},{2,0},{1,5},{5,9},... | collective-permute-start | bytes 1179656 | tf_op jit(solution)/shard_map/ppermute | solution.py:131
  126.2 16.9 %collective-permute-start.24 = (bf16[256,768]{1,0:T(8,128)(2,1)}, bf16[256,768]{1,0:T(8,128)(2,1)}, u32[]{:S(2)}, u32[]{:S(2)}) collective-permute-start(bf16[256,768]{1,0:T(8,128)(2,1)} %collective-permute-done.22), channel_id=1, source_target_pairs={{4,0},{8,4},{12,8},{14,12},{10,14},{6,10},{2,6},{0,2},{5,1},{9,5},... | collective-permute-start | bytes 1179656 | tf_op jit(solution)/shard_map/ppermute | solution.py:132
  133.5 16.9 %collective-permute-start.31 = (bf16[256,768]{1,0:T(8,128)(2,1)}, bf16[256,768]{1,0:T(8,128)(2,1)}, u32[]{:S(2)}, u32[]{:S(2)}) collective-permute-start(bf16[256,768]{1,0:T(8,128)(2,1)} %collective-permute-done.29), channel_id=1, source_target_pairs={{0,4},{4,8},{8,12},{12,14},{14,10},{10,6},{6,2},{2,0},{1,5},{5,9},... | collective-permute-start | bytes 1179656 | tf_op jit(solution)/shard_map/ppermute | solution.py:131
  134.8 17.1 %collective-permute-start.32 = (bf16[256,768]{1,0:T(8,128)(2,1)S(1)}, bf16[256,768]{1,0:T(8,128)(2,1)}, u32[]{:S(2)}, u32[]{:S(2)}) collective-permute-start(bf16[256,768]{1,0:T(8,128)(2,1)S(1)} %collective-permute-done.30), channel_id=1, source_target_pairs={{4,0},{8,4},{12,8},{14,12},{10,14},{6,10},{2,6},{0,2},{5,1},{9,5},... | collective-permute-start | bytes 1179656 | tf_op jit(solution)/shard_map/ppermute | solution.py:132
  151.7 27.5 %collective-permute-start.20 = (bf16[256,1024]{0,1:T(8,128)(2,1)S(1)}, bf16[256,1024]{0,1:T(8,128)(2,1)S(1)}, u32[]{:S(2)}, u32[]{:S(2)}) collective-permute-start(bf16[256,1024]{0,1:T(8,128)(2,1)S(1)} %add_convert_fusion), channel_id=1, source_target_pairs={{0,1},{1,0},{2,3},{3,2},{4,5},{5,4},{6,7},{7,6},{8,9},{9,8},{10,11... | collective-permute-start | bytes 1572872 | tf_op jit(solution)/shard_map/ppermute | solution.py:168
  151.8 26.4 %collective-permute-start.34 = (bf16[256,768]{1,0:T(8,128)(2,1)}, bf16[256,768]{1,0:T(8,128)(2,1)S(1)}, u32[]{:S(2)}, u32[]{:S(2)}) collective-permute-start(bf16[256,768]{1,0:T(8,128)(2,1)} %collective-permute-done.32), channel_id=1, source_target_pairs={{4,0},{8,4},{12,8},{14,12},{10,14},{6,10},{2,6},{0,2},{5,1},{9,5},... | collective-permute-start | bytes 1179656 | tf_op jit(solution)/shard_map/ppermute | solution.py:132
  158.6 17.4 %collective-permute-start.38 = (bf16[128,768]{1,0:T(8,128)(2,1)S(1)}, bf16[128,768]{1,0:T(8,128)(2,1)S(1)}, u32[]{:S(2)}, u32[]{:S(2)}) collective-permute-start(bf16[128,768]{1,0:T(8,128)(2,1)S(1)} %get-tuple-element.7), channel_id=1, source_target_pairs={{0,4},{4,8},{8,12},{12,14},{14,10},{10,6},{6,2},{2,0},{1,5},{5,9},... | collective-permute-start | bytes 589832 | tf_op jit(solution)/shard_map/ppermute | solution.py:146
  159.8 17.3 %collective-permute-start.40 = (bf16[128,768]{1,0:T(8,128)(2,1)S(1)}, bf16[128,768]{1,0:T(8,128)(2,1)S(1)}, u32[]{:S(2)}, u32[]{:S(2)}) collective-permute-start(bf16[128,768]{1,0:T(8,128)(2,1)S(1)} %get-tuple-element.7), channel_id=1, source_target_pairs={{4,0},{8,4},{12,8},{14,12},{10,14},{6,10},{2,6},{0,2},{5,1},{9,5},... | collective-permute-start | bytes 589832 | tf_op jit(solution)/shard_map/ppermute | solution.py:148
  (52 other events, 604.3 us)
